TPU v7x, 512 devices: a whole 4x4x16 slice. The times are simulated.
512 devices in a mesh: ep: 128 (over z, x, core), tp: 4 (over y).
Axes of the slice: x: 4, y: 4, z: 16, core: 2. Of those that a mesh axis runs over, the one named last changes fastest.
Arguments:
- residual_in: bfloat16 [1920, 1536], P('ep'), may hold values from -6 to 6
- rec_state: bfloat16 [1920, 12, 128, 128], P('ep', 'tp'), may hold values from -6 to 6
- mix_gain: float32 [1536], replicated, may hold values from 0.1 to 1.9
- w_query: bfloat16 [1536, 1536], P('tp', 'ep'), may hold values from -0.15625 to 0.15625
- w_forget: bfloat16 [1536, 1536], P('tp', 'ep'), may hold values from -0.15625 to 0.15625
- w_input: bfloat16 [1536, 1536], P('tp', 'ep'), may hold values from -0.15625 to 0.15625
- w_gate: bfloat16 [1536, 1536], P('tp', 'ep'), may hold values from -0.15625 to 0.15625
- lower_bound: float32 [1536], P('tp'), may hold values from 0 to 0.9
- head_gain: float32 [128], replicated, may hold values from 0.1 to 1.9
- w_out: bfloat16 [1536, 1536], P('tp', 'ep'), may hold values from -0.15625 to 0.15625
- ffn_gain: float32 [1536], replicated, may hold values from 0.1 to 1.9
- route_ids: int32 [1920, 6], P('ep'), may hold values from 0 to 127, all different within a row; in each aligned block of 15 rows (0 to 14, 15 to 29, ...) at most 2 rows name the same one
- route_weight: float32 [1920, 6], P('ep'), may hold values from 0.2 to 1
- expert_gate: bfloat16 [128, 1536, 512], P('ep', None, 'tp'), may hold values from -0.15625 to 0.15625
- expert_up: bfloat16 [128, 1536, 512], P('ep', None, 'tp'), may hold values from -0.15625 to 0.15625
- expert_down: bfloat16 [128, 512, 1536], P('ep', 'tp'), may hold values from -0.25 to 0.25
Outputs:
- layer_out: bfloat16 [1920, 1536], P('ep', 'tp')
- new_state: bfloat16 [1920, 12, 128, 128], P('ep', 'tp')
Inputs may be any that keep to these rules, and one draw needn't show every extreme that they name: `route_ids`: each row names 6 different experts. Among the rows of one device no expert is named more than 2 times, and in every draw some device names some expert exactly 2 times.
All inputs are finite; a program needn't handle non-finite values.
Results may differ from a plain program's by a relative error of at most 0.016.
Values may be sent and summed in bfloat16 or wider, within the bound.
A program may use at most 64 MiB of HBM per device.

v0:
```python
import jax
import jax.numpy as jnp
from jax import lax
from jax.sharding import Mesh
from jax.sharding import PartitionSpec as P

EP = ("ep_0", "ep_1", "ep_2")
rms_eps = 1e-06


def in_order(pieces, dim):
    pieces = jnp.moveaxis(pieces, 0, dim)
    shape = pieces.shape
    return pieces.reshape(*shape[:dim], shape[dim] * shape[dim + 1], *shape[dim + 2 :])


def gather_in_order(x, axes, turns):
    pieces = x[None]
    for k in turns:
        pieces = lax.all_gather(pieces, axes[k], axis=0, tiled=True)
    carried = [lax.axis_size(axes[k]) for k in reversed(turns)]
    pieces = pieces.reshape(*carried, *x.shape)
    turned = sorted(range(len(turns)), key=lambda place: turns[len(turns) - 1 - place])
    return pieces.transpose(*turned, *range(len(turns), pieces.ndim)).reshape(-1, *x.shape)


def gather_axes(x, axes, turns, dim):
    return in_order(gather_in_order(x, axes, turns), dim)


def split_up(x, dim, count):
    shape = x.shape
    pieces = x.reshape(*shape[:dim], count, shape[dim] // count, *shape[dim + 1 :])
    return jnp.moveaxis(pieces, dim, 0)


def sent_and_summed(x, axis, dim):
    pieces = split_up(x, dim, lax.axis_size(axis))
    arrived = lax.all_to_all(pieces, axis, split_axis=0, concat_axis=0, tiled=True)
    return arrived.sum(axis=0)


def rms_scale(values, gain):
    return values * lax.rsqrt(jnp.mean(values * values, axis=-1, keepdims=True) + rms_eps) * gain


def rounded(values):
    return lax.optimization_barrier(values.astype(jnp.bfloat16)).astype(jnp.float32)


def recurrence(lower_bound, head_gain, state_block, query_raw, forget_raw, input_raw, gate_raw):
    seq_count = state_block.shape[0]
    heads_local = state_block.shape[1]
    head_size = state_block.shape[2]
    head_shape = (seq_count, heads_local, head_size)
    forget = lower_bound + (1.0 - lower_bound) * jax.nn.sigmoid(forget_raw)
    query_act = jax.nn.silu(query_raw).reshape(head_shape)
    key_act = (1.0 - forget).reshape(head_shape)
    forget_heads = forget.reshape(head_shape)
    value_act = input_raw.reshape(head_shape)
    state_next = (
        forget_heads[:, :, :, None] * state_block.astype(jnp.float32)
        + key_act[:, :, :, None] * value_act[:, :, None, :]
    )
    readout = jnp.einsum("shk,shkv->shv", query_act, state_next, precision=lax.Precision.HIGHEST)
    gate_heads = jax.nn.silu(gate_raw).reshape(head_shape)
    heads_out = rms_scale(readout, head_gain) * gate_heads
    return (
        state_next.astype(jnp.bfloat16),
        heads_out.reshape(seq_count, heads_local * head_size).astype(jnp.bfloat16),
    )


def shards(
    residual_in,
    rec_state,
    mix_gain,
    w_query,
    w_forget,
    w_input,
    w_gate,
    lower_bound,
    head_gain,
    w_out,
    ffn_gain,
    route_ids,
    route_weight,
    expert_gate,
    expert_up,
    expert_down,
):
    tp_count = lax.axis_size("tp")
    tp_rank = lax.axis_index("tp")
    ep_count = lax.axis_size(EP)
    seq_count = residual_in.shape[0]
    model_width = residual_in.shape[1]
    quarter = model_width // tp_count
    residual = residual_in.astype(jnp.float32)
    normed = rms_scale(residual, mix_gain).astype(jnp.bfloat16)
    own_rows = lax.dynamic_slice_in_dim(normed, tp_rank * quarter, quarter, 1)
    rows_piece = gather_axes(own_rows, EP, (0, 1, 2), 0)
    partial_proj = jnp.stack(
        [
            jnp.dot(rows_piece, weight, preferred_element_type=jnp.float32)
            for weight in (w_query, w_forget, w_input, w_gate)
        ],
        axis=1,
    )
    arrived = lax.all_to_all(
        partial_proj.astype(jnp.bfloat16), EP, split_axis=0, concat_axis=2, tiled=True
    ).astype(partial_proj.dtype)
    summed = sent_and_summed(arrived, "tp", 2)
    projected = rounded(summed)
    new_state, heads_out = recurrence(
        lower_bound,
        head_gain,
        rec_state,
        projected[:, 0],
        projected[:, 1],
        projected[:, 2],
        projected[:, 3],
    )
    partial_mix = jnp.dot(
        gather_axes(heads_out, EP, (0, 1, 2), 0), w_out, preferred_element_type=jnp.float32
    )
    mixed_home = lax.all_to_all(
        partial_mix.astype(jnp.bfloat16), EP, split_axis=0, concat_axis=1, tiled=True
    ).astype(partial_mix.dtype)
    mixed = lax.psum(mixed_home.astype(jnp.bfloat16), "tp").astype(jnp.float32)
    after_mix = rounded(residual + mixed)
    normed_ffn = rms_scale(after_mix, ffn_gain).astype(jnp.bfloat16)
    exp_dev = expert_gate.shape[0]
    experts_all = ep_count * exp_dev
    top_count = route_ids.shape[1]
    capacity = max(2, seq_count * top_count // experts_all + 1)
    flat_ids = route_ids.reshape(-1)
    onehot = (flat_ids[:, None] == jnp.arange(experts_all, dtype=jnp.int32)[None, :]).astype(
        jnp.int32
    )
    slot_rank = jnp.sum(jnp.cumsum(onehot, axis=0) * onehot, axis=1) - 1
    slot_index = flat_ids * capacity + slot_rank
    placer_int = (
        jnp.arange(experts_all * capacity, dtype=jnp.int32)[:, None] == slot_index[None, :]
    ).astype(jnp.int32)
    placer = jnp.sum(
        placer_int.reshape(experts_all * capacity, seq_count, top_count), axis=2
    ).astype(jnp.bfloat16)
    buffer = (
        jnp.dot(placer, normed_ffn, preferred_element_type=jnp.float32)
        .astype(jnp.bfloat16)
        .reshape(experts_all, capacity, model_width)
    )
    down_quarter = lax.all_to_all(expert_down, "tp", split_axis=2, concat_axis=1, tiled=True)
    own_quarter = lax.dynamic_slice_in_dim(buffer, tp_rank * quarter, quarter, 2)
    received = lax.all_gather(
        lax.all_to_all(own_quarter, EP, split_axis=0, concat_axis=0, tiled=True),
        "tp",
        axis=2,
        tiled=True,
    )
    slot_count = received.shape[1]
    grouped = received.reshape(ep_count, exp_dev, slot_count, model_width)
    gate_part = jnp.einsum(
        "sjnd,jdf->sjnf", grouped, expert_gate, preferred_element_type=jnp.float32
    )
    up_part = jnp.einsum("sjnd,jdf->sjnf", grouped, expert_up, preferred_element_type=jnp.float32)
    hidden = (jax.nn.silu(gate_part) * up_part).astype(jnp.bfloat16)
    hidden_whole = lax.all_gather(hidden, "tp", axis=3, tiled=True)
    summed_down = jnp.einsum(
        "sjnf,jfd->sjnd", hidden_whole, down_quarter, preferred_element_type=jnp.float32
    )
    returned = summed_down.astype(jnp.bfloat16).reshape(experts_all, slot_count, quarter)
    gathered_back = lax.all_to_all(returned, EP, split_axis=0, concat_axis=0, tiled=True)
    flat_back = gathered_back.reshape(experts_all * capacity, quarter)
    picked = (
        jnp.take(flat_back, slot_index, axis=0)
        .astype(jnp.float32)
        .reshape(seq_count, top_count, quarter)
    )
    expert_sum = jnp.sum(route_weight[:, :, None] * picked, axis=1)
    own_mix = lax.dynamic_slice_in_dim(after_mix, tp_rank * quarter, quarter, 1)
    layer_out = (own_mix + expert_sum).astype(jnp.bfloat16)
    return (layer_out, new_state)


def solution(mesh):
    split = Mesh(mesh.devices.reshape(16, 4, 2, mesh.shape["tp"]), ("ep_0", "ep_1", "ep_2", "tp"))
    in_specs = (
        P(EP, None),
        P(EP, "tp", None, None),
        P(),
        P("tp", EP),
        P("tp", EP),
        P("tp", EP),
        P("tp", EP),
        P("tp"),
        P(),
        P("tp", EP),
        P(),
        P(EP, None),
        P(EP, None),
        P(EP, None, "tp"),
        P(EP, None, "tp"),
        P(EP, "tp", None),
    )
    out_specs = (P(EP, "tp"), P(EP, "tp", None, None))
    return jax.shard_map(
        shards, mesh=split, in_specs=in_specs, out_specs=out_specs, check_vma=False
    )
```

profile of v0, /device:TPU:33, one launch (start us, length us, event | category | flops | bytes accessed | tf_op | source)
XLA Modules:
  0.0 379.6 jit_solution(7095298848502232704)
XLA Ops:
  7.2 0.8 convert_element_type.89
  8.1 0.9 multiply_reduce_fusion.2
  9.0 0.8 dynamic-slice
  9.9 27.1 %all-gather.1 = bf16[16,15,384]{2,1,0:T(8,128)(2,1)S(1)} all-gather(bf16[1,15,384]{2,1,0:T(8,128)(2,1)S(1)} %fusion.28), channel_id=2, replica_groups=mesh['ep_0'=16,'ep_1'=4,'ep_2'=2,'tp'=4] {'ep_0'}, dimensions={0}, use_global_device_ids=true | all-gather | bytes 195840 | tf_op jit(solution)/shard_map/all_gather | solution.py:20
  37.1 11.4 %all_gather.25 = bf16[64,15,384]{2,0,1:T(8,128)(2,1)} all-gather(bf16[16,15,384]{2,0,1:T(8,128)(2,1)S(1)} %copy.112), channel_id=1, replica_groups=mesh['ep_0'=16,'ep_1'=4,'ep_2'=2,'tp'=4] {'ep_1'}, dimensions={0}, use_global_device_ids=true | all-gather | bytes 921600 | tf_op jit(solution)/shard_map/all_gather | solution.py:20
  48.5 27.9 %all-gather.5.cloned.1.call-done = bf16[128,15,384]{2,0,1:T(8,128)(2,1)} async-done(((bf16[64,15,384]{2,0,1:T(8,128)(2,1)}), bf16[128,15,384]{2,0,1:T(8,128)(2,1)}) %all-gather.5.cloned.1.call-update) | async-done | bytes 1474576 | tf_op jit(solution)/shard_map/all_gather | solution.py:20
  76.4 2.2 copy.113
  78.7 0.5 reshape_reshape.6
  80.6 0.5 fusion.4
  81.1 0.5 fusion.5
  81.7 1.3 copy.114
  83.0 2.1 reshape.247
  85.2 35.9 %all_to_all.58 = bf16[128,2,360]{2,1,0:T(2,128)(2,1)S(1)} all-to-all(bf16[128,2,360]{2,1,0:T(2,128)(2,1)S(1)} %reshape.247), channel_id=1, replica_groups=mesh['ep_0'=16,'ep_1'=4,'ep_2'=2,'tp'=4] {'ep_0','ep_1','ep_2'}, dimensions={0} | all-to-all | bytes 368640 | tf_op jit(solution)/shard_map/all_to_all | solution.py:109
  121.0 1.1 reshape.248
  122.1 2.0 copy.115
  124.1 4.1 %reshape.222 = f32[128,15,4,12]{1,0,2,3:T(8,128)S(1)} reshape(bf16[1920,4,12]{0,1,2:T(4,128)(2,1)} %copy.115) | data formatting | bytes 552960 | tf_op jit(solution)/shard_map/transpose | solution.py:34
  128.3 6.1 %copy.116 = f32[15,4,128,12]{3,2,1,0:T(8,128)} copy(f32[15,4,128,12]{0,2,1,3:T(8,128)S(1)} %bitcast.98) | data formatting | bytes 737280 | tf_op jit(solution)/shard_map/transpose | solution.py:34
  134.4 4.8 %reshape.221 = f32[15,4,4,384]{3,2,1,0:T(4,128)S(1)} reshape(f32[15,4,128,12]{3,2,1,0:T(8,128)} %copy.116) | data formatting | bytes 737280 | tf_op jit(solution)/shard_map/transpose | solution.py:34
  139.2 0.8 copy.117
  140.1 4.0 %all-to-all-start.1 = ((f32[4,15,4,384]{3,2,1,0:T(4,128)}), f32[4,15,4,384]{3,2,1,0:T(4,128)S(1)}, u32[]{:S(2)}, u32[]{:S(2)}) async-start(f32[4,15,4,384]{3,2,1,0:T(4,128)} %copy.117), calls=%async_computation.1 | async-start | bytes 737280 | tf_op jit(solution)/shard_map/all_to_all | solution.py:39
  144.1 6.9 %all-to-all-done.1 = f32[4,15,4,384]{3,2,1,0:T(4,128)S(1)} async-done(((f32[4,15,4,384]{3,2,1,0:T(4,128)}), f32[4,15,4,384]{3,2,1,0:T(4,128)S(1)}, u32[]{:S(2)}, u32[]{:S(2)}) %all-to-all-start.1) | async-done | bytes 368672 | tf_op jit(solution)/shard_map/all_to_all | solution.py:39
  151.5 4.0 %fusion.1 = f32[15,3,1,128]{3,2,1,0:T(1,128)S(1)} fusion(bf16[15,3,128,128]{3,2,1,0:T(8,128)(2,1)S(1)} %copy-done.1, f32[15,3,128]{2,1,0:T(4,128)S(1)} %mul.168, f32[15,3,128]{2,1,0:T(4,128)S(1)} %get-tuple-element.8, f32[15,3,128]{2,1,0:T(4,128)S(1)} %get-tuple-element.9, f32[15,3,128,1]{2,1,0,3:T(4,128)S(1)} %fusion.21), kind=kOutput, calls=%fused_computation.3 | convolution fusion | flops 11796480 | bytes 1589760 | tf_op jit(solution)/shard_map/shk,shkv->shv/dot_general | solution.py:65
  155.7 19.8 %all_gather.27 = bf16[16,15,384]{2,1,0:T(8,128)(2,1)S(1)} all-gather(bf16[1,15,384]{2,1,0:T(8,128)(2,1)S(1)} %convert_element_type.98), channel_id=1, replica_groups=mesh['ep_0'=16,'ep_1'=4,'ep_2'=2,'tp'=4] {'ep_0'}, dimensions={0}, use_global_device_ids=true | all-gather | bytes 195840 | tf_op jit(solution)/shard_map/all_gather | solution.py:20
  175.6 11.5 %all_gather.28 = bf16[64,15,384]{2,0,1:T(8,128)(2,1)} all-gather(bf16[16,15,384]{2,0,1:T(8,128)(2,1)S(1)} %copy.119), channel_id=1, replica_groups=mesh['ep_0'=16,'ep_1'=4,'ep_2'=2,'tp'=4] {'ep_1'}, dimensions={0}, use_global_device_ids=true | all-gather | bytes 921600 | tf_op jit(solution)/shard_map/all_gather | solution.py:20
  187.8 22.7 %all-gather.7.cloned.1.call-done = bf16[128,15,384]{2,0,1:T(8,128)(2,1)} async-done(((bf16[64,15,384]{2,0,1:T(8,128)(2,1)}), bf16[128,15,384]{2,0,1:T(8,128)(2,1)}) %all-gather.7.cloned.1.call-update) | async-done | bytes 1474576 | tf_op jit(solution)/shard_map/all_gather | solution.py:20
  210.4 2.2 copy.149
  213.2 1.2 convolution_convert_fusion.1
  214.4 0.8 all_to_all.43
  215.2 1.1 copy.121
  216.3 16.2 %all-to-all-start.2 = ((bf16[128,15,12]{1,2,0:T(8,128)(2,1)}), bf16[128,15,12]{1,2,0:T(8,128)(2,1)S(1)}, u32[]{:S(2)}, u32[]{:S(2)}) async-start(bf16[128,15,12]{1,2,0:T(8,128)(2,1)} %copy.121), calls=%async_computation.2 | async-start | bytes 1048576 | tf_op jit(solution)/shard_map/all_to_all | solution.py:126
  232.6 0.6 copy.128
  233.2 0.5 broadcast.193
  233.7 8.8 %reduce.8 = bf16[1536,128]{1,0:T(8,128)(2,1)S(1)} reduce(bf16[1536,1,128]{2,1,0:T(2,128)(2,1)S(1)} %bitcast.100, bf16[]{:T(256)} %broadcast.193), dimensions={1}, to_apply=%bitcast.82.reduce_sub_computation | reduce | bytes 786434
  242.5 0.8 reshape.245
  243.5 22.8 %all-to-all-done.2 = bf16[128,15,12]{1,2,0:T(8,128)(2,1)S(1)} async-done(((bf16[128,15,12]{1,2,0:T(8,128)(2,1)}), bf16[128,15,12]{1,2,0:T(8,128)(2,1)S(1)}, u32[]{:S(2)}, u32[]{:S(2)}) %all-to-all-start.2) | async-done | bytes 46112 | tf_op jit(solution)/shard_map/all_to_all | solution.py:126
  266.2 4.0 %all-to-all-start.4 = ((bf16[4,2,24576]{2,1,0:T(2,128)(2,1)}), bf16[4,2,24576]{2,1,0:T(2,128)(2,1)S(1)}, u32[]{:S(2)}, u32[]{:S(2)}) async-start(bf16[4,2,24576]{2,1,0:T(2,128)(2,1)} %reshape.245), calls=%async_computation.4 | async-start | bytes 786432 | tf_op jit(solution)/shard_map/all_to_all | solution.py:153
  270.6 14.8 %psum.7 = bf16[15,1536]{1,0:T(8,128)(2,1)S(1)} all-reduce(bf16[15,1536]{1,0:T(8,128)(2,1)S(1)} %copy.133), channel_id=1, replica_groups=mesh['ep_0'=16,'ep_1'=4,'ep_2'=2,'tp'=4] {'tp'}, use_global_device_ids=true, to_apply=%region_3.4 | all-reduce | flops 23040 | bytes 92160 | tf_op jit(solution)/shard_map/psum | solution.py:129
  286.3 0.8 constant_dynamic-slice_fusion
  287.1 9.6 %all-to-all-start.3 = ((bf16[128,2,384]{2,1,0:T(2,128)(2,1)}), bf16[128,2,384]{2,1,0:T(2,128)(2,1)S(1)}, u32[]{:S(2)}, u32[]{:S(2)}) async-start(bf16[128,2,384]{2,1,0:T(2,128)(2,1)} %constant_dynamic-slice_fusion), calls=%async_computation.3 | async-start | bytes 393216 | tf_op jit(solution)/shard_map/all_to_all | solution.py:156
  297.4 19.0 %all-to-all-done.3 = bf16[128,2,384]{2,1,0:T(2,128)(2,1)S(1)} async-done(((bf16[128,2,384]{2,1,0:T(2,128)(2,1)}), bf16[128,2,384]{2,1,0:T(2,128)(2,1)S(1)}, u32[]{:S(2)}, u32[]{:S(2)}) %all-to-all-start.3) | async-done | bytes 196640 | tf_op jit(solution)/shard_map/all_to_all | solution.py:156
  316.4 11.6 %all_gather.30 = bf16[128,2,1536]{2,0,1:T(8,128)(2,1)S(1)} all-gather(bf16[128,2,384]{2,0,1:T(8,128)(2,1)S(1)} %copy.127), channel_id=1, replica_groups=mesh['ep_0'=16,'ep_1'=4,'ep_2'=2,'tp'=4] {'tp'}, dimensions={2}, use_global_device_ids=true | all-gather | bytes 983040 | tf_op jit(solution)/shard_map/all_gather | solution.py:155
  328.8 9.7 %all_gather.31 = bf16[128,1,2,512]{3,0,2,1:T(8,128)(2,1)S(1)} all-gather(bf16[128,1,2,128]{3,0,2,1:T(8,128)(2,1)S(1)} %fusion.10), channel_id=1, replica_groups=mesh['ep_0'=16,'ep_1'=4,'ep_2'=2,'tp'=4] {'tp'}, dimensions={3}, use_global_device_ids=true | all-gather | bytes 327680 | tf_op jit(solution)/shard_map/all_gather | solution.py:168
  338.9 0.9 copy.130
  339.7 11.6 %all-to-all-start.5 = ((bf16[128,2,384]{2,1,0:T(2,128)(2,1)}), bf16[128,2,384]{2,1,0:T(2,128)(2,1)S(1)}, u32[]{:S(2)}, u32[]{:S(2)}) async-start(bf16[128,2,384]{2,1,0:T(2,128)(2,1)} %copy.130), calls=%async_computation.5 | async-start | bytes 393216 | tf_op jit(solution)/shard_map/all_to_all | solution.py:173
  351.6 2.9 fusion
  354.5 16.7 %all-to-all-done.5 = bf16[128,2,384]{2,1,0:T(2,128)(2,1)S(1)} async-done(((bf16[128,2,384]{2,1,0:T(2,128)(2,1)}), bf16[128,2,384]{2,1,0:T(2,128)(2,1)S(1)}, u32[]{:S(2)}, u32[]{:S(2)}) %all-to-all-start.5) | async-done | bytes 196640 | tf_op jit(solution)/shard_map/all_to_all | solution.py:173
  371.2 0.8 gather_fusion
  372.2 0.6 add_convert_fusion.1
  (94 shorter events, 7.2 us)
Async XLA Ops:
  7.2 320.9 %copy-start = (bf16[1,1536,128]{2,1,0:T(8,128)(2,1)S(1)}, bf16[1,1536,128]{2,1,0:T(8,128)(2,1)}, u32[]{:S(2)}) copy-start(bf16[1,1536,128]{2,1,0:T(8,128)(2,1)} %param.29) | copy-start | bytes 1179652
  7.2 69.2 %all-gather.5.cloned.1.call-start = ((), (), s32[]{:S(2)}) async-start(), calls=%async_computation.6 | async-start | bytes 2211840 | tf_op jit(solution)/shard_map/all_gather | solution.py:20
  78.7 0.7 copy-start.5
  79.4 0.7 copy-start.6
  79.4 1.2 copy-start.7
  80.1 1.0 copy-start.8
  134.4 9.7 %copy-start.10 = (f32[384]{0:T(512)S(1)}, f32[384]{0:T(512)}, u32[]{:S(2)}) copy-start(f32[384]{0:T(512)} %param.23) | copy-start | bytes 4612
  139.2 12.3 %copy-start.1 = (bf16[15,3,128,128]{3,2,1,0:T(8,128)(2,1)S(1)}, bf16[15,3,128,128]{3,2,1,0:T(8,128)(2,1)}, u32[]{:S(2)}) copy-start(bf16[15,3,128,128]{3,2,1,0:T(8,128)(2,1)} %param.17) | copy-start | bytes 4423684
  140.1 10.9 %all-to-all-start.1 = ((f32[4,15,4,384]{3,2,1,0:T(4,128)}), f32[4,15,4,384]{3,2,1,0:T(4,128)S(1)}, u32[]{:S(2)}, u32[]{:S(2)}) async-start(f32[4,15,4,384]{3,2,1,0:T(4,128)} %copy.117), calls=%async_computation.1 | async-start | bytes 737280 | tf_op jit(solution)/shard_map/all_to_all | solution.py:39
  144.1 66.4 %all-gather.7.cloned.1.call-start = ((), (), s32[]{:S(2)}) async-start(), calls=%async_computation.7 | async-start | bytes 2211840 | tf_op jit(solution)/shard_map/all_gather | solution.py:20
  151.5 4.1 %copy-start.13 = (f32[128]{0:T(128)S(1)}, f32[128]{0:T(128)}, u32[]{:S(2)}) copy-start(f32[128]{0:T(128)} %param.24) | copy-start | bytes 1540
  155.5 31.6 %copy-start.11 = (s32[15,6]{0,1:T(8,128)S(1)}, s32[15,6]{0,1:T(8,128)}, u32[]{:S(2)}) copy-start(s32[15,6]{0,1:T(8,128)} %param.27) | copy-start | bytes 1084
  187.7 22.8 %copy-start.14 = (s32[90]{0:T(128)}, s32[90]{0:T(128)S(1)}, u32[]{:S(2)}) copy-start(s32[90]{0:T(128)S(1)} %select_reduce_fusion) | copy-start | bytes 1084
  214.4 18.2 %copy-start.4 = (bf16[1,128,1536]{2,1,0:T(8,128)(2,1)S(1)}, bf16[1,128,1536]{2,1,0:T(8,128)(2,1)}, u32[]{:S(2)}) copy-start(bf16[1,128,1536]{2,1,0:T(8,128)(2,1)} %param.31) | copy-start | bytes 1179652
  216.3 50.0 %all-to-all-start.2 = ((bf16[128,15,12]{1,2,0:T(8,128)(2,1)}), bf16[128,15,12]{1,2,0:T(8,128)(2,1)S(1)}, u32[]{:S(2)}, u32[]{:S(2)}) async-start(bf16[128,15,12]{1,2,0:T(8,128)(2,1)} %copy.121), calls=%async_computation.2 | async-start | bytes 1048576 | tf_op jit(solution)/shard_map/all_to_all | solution.py:126
  242.5 42.9 %copy-start.3 = (bf16[15,1536]{1,0:T(8,128)(2,1)S(1)}, bf16[15,1536]{1,0:T(8,128)(2,1)}, u32[]{:S(2)}) copy-start(bf16[15,1536]{1,0:T(8,128)(2,1)} %param.16) | copy-start | bytes 138244
  242.5 43.0 %copy-start.9 = (f32[1536]{0:T(1024)S(1)}, f32[1536]{0:T(1024)}, u32[]{:S(2)}) copy-start(f32[1536]{0:T(1024)} %param.26) | copy-start | bytes 18436
  266.2 20.9 %all-to-all-start.4 = ((bf16[4,2,24576]{2,1,0:T(2,128)(2,1)}), bf16[4,2,24576]{2,1,0:T(2,128)(2,1)S(1)}, u32[]{:S(2)}, u32[]{:S(2)}) async-start(bf16[4,2,24576]{2,1,0:T(2,128)(2,1)} %reshape.245), calls=%async_computation.4 | async-start | bytes 786432 | tf_op jit(solution)/shard_map/all_to_all | solution.py:153
  287.1 29.3 %all-to-all-start.3 = ((bf16[128,2,384]{2,1,0:T(2,128)(2,1)}), bf16[128,2,384]{2,1,0:T(2,128)(2,1)S(1)}, u32[]{:S(2)}, u32[]{:S(2)}) async-start(bf16[128,2,384]{2,1,0:T(2,128)(2,1)} %constant_dynamic-slice_fusion), calls=%async_computation.3 | async-start | bytes 393216 | tf_op jit(solution)/shard_map/all_to_all | solution.py:156
  297.4 31.1 %copy-start.16 = (bf16[1,1536,128]{2,1,0:T(8,128)(2,1)S(1)}, bf16[1,1536,128]{2,1,0:T(8,128)(2,1)}, u32[]{:S(2)}) copy-start(bf16[1,1536,128]{2,1,0:T(8,128)(2,1)} %param.30) | copy-start | bytes 1179652
  328.4 23.0 %copy-start.12 = (f32[15,6]{0,1:T(8,128)S(1)}, f32[15,6]{0,1:T(8,128)}, u32[]{:S(2)}) copy-start(f32[15,6]{0,1:T(8,128)} %param.28) | copy-start | bytes 1084
  328.5 23.1 %copy-start.15 = (s32[90]{0:T(128)S(1)}, s32[90]{0:T(128)}, u32[]{:S(2)}) copy-start(s32[90]{0:T(128)} %copy-done.14) | copy-start | bytes 1084
  328.5 23.1 %copy-start.2 = (bf16[15,3,128,128]{3,2,1,0:T(8,128)(2,1)S(1)}, bf16[15,3,128,128]{3,2,1,0:T(8,128)(2,1)}, u32[]{:S(2)}) copy-start(bf16[15,3,128,128]{3,2,1,0:T(8,128)(2,1)} %param.17) | copy-start | bytes 4423684
  339.7 31.4 %all-to-all-start.5 = ((bf16[128,2,384]{2,1,0:T(2,128)(2,1)}), bf16[128,2,384]{2,1,0:T(2,128)(2,1)S(1)}, u32[]{:S(2)}, u32[]{:S(2)}) async-start(bf16[128,2,384]{2,1,0:T(2,128)(2,1)} %copy.130), calls=%async_computation.5 | async-start | bytes 393216 | tf_op jit(solution)/shard_map/all_to_all | solution.py:173
Sparse Core Ops, SparseCore 0:
  48.6 27.7 all-gather.4
  187.2 23.1 all-gather.6
where the time goes:
time: 381 us; the launch traced here: 380 us
  blocking collectives  142 us (37%)
  waiting for transfers between devices  116 us (30%)
  starting transfers between devices  45.5 us (12%)
  local copies, waits for them, and re-layouts  37.6 us (10%)
  other arithmetic  15.6 us (4%)
  between operations  14.5 us (4%)
  matrix products  8.61 us (2%)
    all_gather x4, blocking collectives, gather_in_order(): pieces = lax.all_gather(pieces, axes[k], axis=0, tiled=True)  69.9 us
    all_gather x2, waiting for transfers between devices, gather_in_order(): pieces = lax.all_gather(pieces, axes[k], axis=0, tiled=True)  50.6 us
    all_to_all x1, blocking collectives, shards(): lax.all_to_all(partial_proj.astype(jnp.bfloat16), EP, split_axis=0, conca...  35.9 us
    all_to_all x1, waiting for transfers between devices, shards(): lax.all_to_all(partial_mix.astype(jnp.bfloat16), EP, split_axis=0, concat...  22.8 us
    all_to_all x1, waiting for transfers between devices, shards(): lax.all_to_all(own_quarter, EP, split_axis=0, concat_axis=0, tiled=True)  19 us
    all_to_all x1, waiting for transfers between devices, shards(): lax.all_to_all(returned, EP, split_axis=0, concat_axis=0, tiled=True)  16.7 us
    all_to_all x1, starting transfers between devices, shards(): lax.all_to_all(partial_mix.astype(jnp.bfloat16), EP, split_axis=0, concat...  16.2 us
    transpose x4, local copies, waits for them, and re-layouts, split_up(): return jnp.moveaxis(pieces, dim, 0)  15.9 us
  transfers between devices with their start and end apart: 7, of which 6 were waited for; matrix products, arithmetic and copies ran while one was open for 5% of the time, Pallas kernels for 0%

commit v1 on v0

--- a/solution.py
+++ b/solution.py
@@ -8,6 +8,11 @@
 rms_eps = 1e-06
 
 
+def exchange_gather(array, axis, d):
+    sent = jnp.stack([array] * lax.axis_size(axis))
+    return jnp.concatenate(lax.all_to_all(sent, axis, 0, 0), axis=d)
+
+
 def in_order(pieces, dim):
     pieces = jnp.moveaxis(pieces, 0, dim)
     shape = pieces.shape
@@ -17,7 +22,7 @@
 def gather_in_order(x, axes, turns):
     pieces = x[None]
     for k in turns:
-        pieces = lax.all_gather(pieces, axes[k], axis=0, tiled=True)
+        pieces = exchange_gather(pieces, axes[k], 0)
     carried = [lax.axis_size(axes[k]) for k in reversed(turns)]
     pieces = pieces.reshape(*carried, *x.shape)
     turned = sorted(range(len(turns)), key=lambda place: turns[len(turns) - 1 - place])

time: 381 us -> 320 us (0.84)
  waiting for transfers between devices: 116 us -> 87.9 us
  blocking collectives: 142 us -> 124 us
  between operations: 14.5 us -> 1.23 us
    all_gather x4 -> x0, blocking collectives: 69.9 us -> none  [gather_in_order(): pieces = lax.all_gather(pieces, axes[k], axis=0, tiled=True)]
    all_to_all x0 -> x4, blocking collectives: none -> 60.1 us  [exchange_gather(): return jnp.concatenate(lax.all_to_all(sent, axis, 0, 0), axis=d)]
    all_gather x2 -> x0, waiting for transfers between devices: 50.6 us -> none  [gather_in_order(): pieces = lax.all_gather(pieces, axes[k], axis=0, tiled=True)]
    all_to_all x0 -> x2, waiting for transfers between devices: none -> 22.5 us  [exchange_gather(): return jnp.concatenate(lax.all_to_all(sent, axis, 0, 0), axis=d)]
    all_to_all x1, blocking collectives: 35.9 us -> 27.6 us  [shards(): lax.all_to_all(partial_proj.astype(jnp.bfloat16), EP, split_axis=0, conca...]
    all_to_all x1, starting transfers between devices: 16.2 us -> 8.31 us  [shards(): lax.all_to_all(partial_mix.astype(jnp.bfloat16), EP, split_axis=0, concat...]
    all_to_all x0 -> x2, starting transfers between devices: none -> 7.6 us  [exchange_gather(): return jnp.concatenate(lax.all_to_all(sent, axis, 0, 0), axis=d)]
    unnamed x2 -> x1, other arithmetic: 8.88 us -> 8.8 us
where the time goes in v1:
time: 320 us; the launch traced here: 319 us
  blocking collectives  124 us (39%)
  waiting for transfers between devices  87.9 us (27%)
  starting transfers between devices  44 us (14%)
  local copies, waits for them, and re-layouts  36.7 us (11%)
  other arithmetic  15.9 us (5%)
  matrix products  8.61 us (3%)
    all_to_all x4, blocking collectives, exchange_gather(): return jnp.concatenate(lax.all_to_all(sent, axis, 0, 0), axis=d)  60.1 us
    all_to_all x1, blocking collectives, shards(): lax.all_to_all(partial_proj.astype(jnp.bfloat16), EP, split_axis=0, conca...  27.6 us
    all_to_all x1, waiting for transfers between devices, shards(): lax.all_to_all(partial_mix.astype(jnp.bfloat16), EP, split_axis=0, concat...  22.8 us
    all_to_all x2, waiting for transfers between devices, exchange_gather(): return jnp.concatenate(lax.all_to_all(sent, axis, 0, 0), axis=d)  22.5 us
    all_to_all x1, waiting for transfers between devices, shards(): lax.all_to_all(own_quarter, EP, split_axis=0, concat_axis=0, tiled=True)  19 us
    all_to_all x1, waiting for transfers between devices, shards(): lax.all_to_all(returned, EP, split_axis=0, concat_axis=0, tiled=True)  16.7 us
    transpose x4, local copies, waits for them, and re-layouts, split_up(): return jnp.moveaxis(pieces, dim, 0)  15.9 us
    psum x1, blocking collectives, shards(): mixed = lax.psum(mixed_home.astype(jnp.bfloat16), 'tp').astype(jnp.float32)  15.3 us
  transfers between devices with their start and end apart: 7, of which 6 were waited for; matrix products, arithmetic and copies ran while one was open for 5% of the time, Pallas kernels for 0%

profile of v1, /device:TPU:33, one launch (start us, length us, event | category | flops | bytes accessed | tf_op | source)
XLA Modules:
  0.0 318.5 jit_solution(12783861820397967200)
XLA Ops:
  0.6 0.9 convert_element_type.87
  1.5 0.9 multiply_reduce_fusion.2
  2.4 0.8 dynamic-slice
  3.3 30.4 %all_to_all.88 = bf16[16,1,15,384]{3,2,1,0:T(8,128)(2,1)S(1)} all-to-all(bf16[16,1,15,384]{3,2,1,0:T(8,128)(2,1)S(1)} %stack.38), channel_id=1, replica_groups=mesh['ep_0'=16,'ep_1'=4,'ep_2'=2,'tp'=4] {'ep_0'}, dimensions={0} | all-to-all | bytes 368640 | tf_op jit(solution)/shard_map/all_to_all | solution.py:13
  33.8 14.2 %all_to_all.89 = bf16[4,16,15,384]{3,1,2,0:T(8,128)(2,1)S(1)} all-to-all(bf16[4,16,15,384]{3,1,2,0:T(8,128)(2,1)S(1)} %stack.39), channel_id=1, replica_groups=mesh['ep_0'=16,'ep_1'=4,'ep_2'=2,'tp'=4] {'ep_1'}, dimensions={0} | all-to-all | bytes 1474560 | tf_op jit(solution)/shard_map/all_to_all | solution.py:13
  48.3 6.9 %all_to_all.90 = bf16[2,64,15,384]{3,1,2,0:T(8,128)(2,1)S(1)} all-to-all(bf16[2,64,15,384]{3,1,2,0:T(8,128)(2,1)S(1)} %pad_maximum_fusion), channel_id=1, replica_groups=mesh['ep_0'=16,'ep_1'=4,'ep_2'=2,'tp'=4] {'ep_2'}, dimensions={0} | all-to-all | bytes 2949120 | tf_op jit(solution)/shard_map/all_to_all | solution.py:13
  55.1 0.9 copy.107
  59.1 1.3 copy.108
  60.4 2.1 reshape.239
  62.5 27.6 %all_to_all.91 = bf16[128,2,360]{2,1,0:T(2,128)(2,1)S(1)} all-to-all(bf16[128,2,360]{2,1,0:T(2,128)(2,1)S(1)} %reshape.239), channel_id=1, replica_groups=mesh['ep_0'=16,'ep_1'=4,'ep_2'=2,'tp'=4] {'ep_0','ep_1','ep_2'}, dimensions={0} | all-to-all | bytes 368640 | tf_op jit(solution)/shard_map/all_to_all | solution.py:114
  90.1 1.1 reshape.240
  91.2 2.0 copy.109
  93.2 4.1 %reshape.218 = f32[128,15,4,12]{1,0,2,3:T(8,128)S(1)} reshape(bf16[1920,4,12]{0,1,2:T(4,128)(2,1)} %copy.109) | data formatting | bytes 552960 | tf_op jit(solution)/shard_map/transpose | solution.py:39
  97.3 6.1 %copy.110 = f32[15,4,128,12]{3,2,1,0:T(8,128)} copy(f32[15,4,128,12]{0,2,1,3:T(8,128)S(1)} %bitcast.102) | data formatting | bytes 737280 | tf_op jit(solution)/shard_map/transpose | solution.py:39
  103.4 4.8 %reshape.217 = f32[15,4,4,384]{3,2,1,0:T(4,128)S(1)} reshape(f32[15,4,128,12]{3,2,1,0:T(8,128)} %copy.110) | data formatting | bytes 737280 | tf_op jit(solution)/shard_map/transpose | solution.py:39
  108.3 0.8 copy.111
  109.1 4.2 %all-to-all-start.4 = ((f32[4,15,4,384]{3,2,1,0:T(4,128)}), f32[4,15,4,384]{3,2,1,0:T(4,128)S(1)}, u32[]{:S(2)}, u32[]{:S(2)}) async-start(f32[4,15,4,384]{3,2,1,0:T(4,128)} %copy.111), calls=%async_computation.4 | async-start | bytes 737280 | tf_op jit(solution)/shard_map/all_to_all | solution.py:44
  113.3 6.9 %all-to-all-done.4 = f32[4,15,4,384]{3,2,1,0:T(4,128)S(1)} async-done(((f32[4,15,4,384]{3,2,1,0:T(4,128)}), f32[4,15,4,384]{3,2,1,0:T(4,128)S(1)}, u32[]{:S(2)}, u32[]{:S(2)}) %all-to-all-start.4) | async-done | bytes 368672 | tf_op jit(solution)/shard_map/all_to_all | solution.py:44
  120.7 4.0 %fusion.1 = f32[15,3,1,128]{3,2,1,0:T(1,128)S(1)} fusion(bf16[15,3,128,128]{3,2,1,0:T(8,128)(2,1)S(1)} %copy-done.1, f32[15,3,128]{2,1,0:T(4,128)S(1)} %mul.168, f32[15,3,128]{2,1,0:T(4,128)S(1)} %get-tuple-element.8, f32[15,3,128]{2,1,0:T(4,128)S(1)} %get-tuple-element.9, f32[15,3,128,1]{2,1,0,3:T(4,128)S(1)} %fusion.21), kind=kOutput, calls=%fused_computation.3 | convolution fusion | flops 11796480 | bytes 1589760 | tf_op jit(solution)/shard_map/shk,shkv->shv/dot_general | solution.py:70
  125.0 0.7 stack.46
  125.7 3.6 %all-to-all-start.5 = ((bf16[16,1,15,384]{3,2,1,0:T(8,128)(2,1)}), bf16[16,1,15,384]{3,2,1,0:T(8,128)(2,1)S(1)}, u32[]{:S(2)}, u32[]{:S(2)}) async-start(bf16[16,1,15,384]{3,2,1,0:T(8,128)(2,1)} %stack.46), calls=%async_computation.5 | async-start | bytes 393216 | tf_op jit(solution)/shard_map/all_to_all | solution.py:13
  129.4 14.4 %all-to-all-done.5 = bf16[16,1,15,384]{3,2,1,0:T(8,128)(2,1)S(1)} async-done(((bf16[16,1,15,384]{3,2,1,0:T(8,128)(2,1)}), bf16[16,1,15,384]{3,2,1,0:T(8,128)(2,1)S(1)}, u32[]{:S(2)}, u32[]{:S(2)}) %all-to-all-start.5) | async-done | bytes 184352 | tf_op jit(solution)/shard_map/all_to_all | solution.py:13
  143.9 0.9 stack.47
  144.8 4.0 %all-to-all-start.6 = ((bf16[4,16,15,384]{3,1,2,0:T(8,128)(2,1)}), bf16[4,16,15,384]{3,1,2,0:T(8,128)(2,1)S(1)}, u32[]{:S(2)}, u32[]{:S(2)}) async-start(bf16[4,16,15,384]{3,1,2,0:T(8,128)(2,1)} %stack.47), calls=%async_computation.6 | async-start | bytes 1474560 | tf_op jit(solution)/shard_map/all_to_all | solution.py:13
  149.3 8.1 %all-to-all-done.6 = bf16[4,16,15,384]{3,1,2,0:T(8,128)(2,1)S(1)} async-done(((bf16[4,16,15,384]{3,1,2,0:T(8,128)(2,1)}), bf16[4,16,15,384]{3,1,2,0:T(8,128)(2,1)S(1)}, u32[]{:S(2)}, u32[]{:S(2)}) %all-to-all-start.6) | async-done | bytes 737312 | tf_op jit(solution)/shard_map/all_to_all | solution.py:13
  157.7 8.7 %all_to_all.92 = bf16[2,64,15,384]{3,1,2,0:T(8,128)(2,1)S(1)} all-to-all(bf16[2,64,15,384]{3,1,2,0:T(8,128)(2,1)S(1)} %pad_maximum_fusion.1), channel_id=1, replica_groups=mesh['ep_0'=16,'ep_1'=4,'ep_2'=2,'tp'=4] {'ep_2'}, dimensions={0} | all-to-all | bytes 2949120 | tf_op jit(solution)/shard_map/all_to_all | solution.py:13
  166.3 0.9 copy.115
  167.7 1.2 convolution_convert_fusion.1
  168.9 0.8 all_to_all.67
  169.7 1.1 copy.116
  170.8 8.3 %all-to-all-start.8 = ((bf16[128,15,12]{1,2,0:T(8,128)(2,1)}), bf16[128,15,12]{1,2,0:T(8,128)(2,1)S(1)}, u32[]{:S(2)}, u32[]{:S(2)}) async-start(bf16[128,15,12]{1,2,0:T(8,128)(2,1)} %copy.116), calls=%async_computation.8 | async-start | bytes 1048576 | tf_op jit(solution)/shard_map/all_to_all | solution.py:131
  179.2 0.6 copy.123
  180.3 8.8 %reduce.8 = bf16[1536,128]{1,0:T(8,128)(2,1)S(1)} reduce(bf16[1536,1,128]{2,1,0:T(2,128)(2,1)S(1)} %bitcast.105, bf16[]{:T(256)} %broadcast.199), dimensions={1}, to_apply=%bitcast.87.reduce_sub_computation | reduce | bytes 786434
  189.2 0.8 reshape.237
  190.1 22.8 %all-to-all-done.8 = bf16[128,15,12]{1,2,0:T(8,128)(2,1)S(1)} async-done(((bf16[128,15,12]{1,2,0:T(8,128)(2,1)}), bf16[128,15,12]{1,2,0:T(8,128)(2,1)S(1)}, u32[]{:S(2)}, u32[]{:S(2)}) %all-to-all-start.8) | async-done | bytes 46112 | tf_op jit(solution)/shard_map/all_to_all | solution.py:131
  212.8 3.5 %all-to-all-start.10 = ((bf16[4,2,24576]{2,1,0:T(2,128)(2,1)}), bf16[4,2,24576]{2,1,0:T(2,128)(2,1)S(1)}, u32[]{:S(2)}, u32[]{:S(2)}) async-start(bf16[4,2,24576]{2,1,0:T(2,128)(2,1)} %reshape.237), calls=%async_computation.10 | async-start | bytes 786432 | tf_op jit(solution)/shard_map/all_to_all | solution.py:158
  216.7 15.3 %psum.7 = bf16[15,1536]{1,0:T(8,128)(2,1)S(1)} all-reduce(bf16[15,1536]{1,0:T(8,128)(2,1)S(1)} %copy.128), channel_id=1, replica_groups=mesh['ep_0'=16,'ep_1'=4,'ep_2'=2,'tp'=4] {'tp'}, use_global_device_ids=true, to_apply=%region_3.4 | all-reduce | flops 23040 | bytes 92160 | tf_op jit(solution)/shard_map/psum | solution.py:134
  232.8 0.8 constant_dynamic-slice_fusion
  233.6 8.8 %all-to-all-start.9 = ((bf16[128,2,384]{2,1,0:T(2,128)(2,1)}), bf16[128,2,384]{2,1,0:T(2,128)(2,1)S(1)}, u32[]{:S(2)}, u32[]{:S(2)}) async-start(bf16[128,2,384]{2,1,0:T(2,128)(2,1)} %constant_dynamic-slice_fusion), calls=%async_computation.9 | async-start | bytes 393216 | tf_op jit(solution)/shard_map/all_to_all | solution.py:161
  243.1 19.0 %all-to-all-done.9 = bf16[128,2,384]{2,1,0:T(2,128)(2,1)S(1)} async-done(((bf16[128,2,384]{2,1,0:T(2,128)(2,1)}), bf16[128,2,384]{2,1,0:T(2,128)(2,1)S(1)}, u32[]{:S(2)}, u32[]{:S(2)}) %all-to-all-start.9) | async-done | bytes 196640 | tf_op jit(solution)/shard_map/all_to_all | solution.py:161
  262.2 11.6 %all_gather.6 = bf16[128,2,1536]{2,0,1:T(8,128)(2,1)S(1)} all-gather(bf16[128,2,384]{2,0,1:T(8,128)(2,1)S(1)} %copy.122), channel_id=1, replica_groups=mesh['ep_0'=16,'ep_1'=4,'ep_2'=2,'tp'=4] {'tp'}, dimensions={2}, use_global_device_ids=true | all-gather | bytes 983040 | tf_op jit(solution)/shard_map/all_gather | solution.py:160
  274.6 9.7 %all_gather.7 = bf16[128,1,2,512]{3,0,2,1:T(8,128)(2,1)S(1)} all-gather(bf16[128,1,2,128]{3,0,2,1:T(8,128)(2,1)S(1)} %fusion.10), channel_id=1, replica_groups=mesh['ep_0'=16,'ep_1'=4,'ep_2'=2,'tp'=4] {'tp'}, dimensions={3}, use_global_device_ids=true | all-gather | bytes 327680 | tf_op jit(solution)/shard_map/all_gather | solution.py:173
  284.6 0.9 copy.125
  285.5 11.6 %all-to-all-start.11 = ((bf16[128,2,384]{2,1,0:T(2,128)(2,1)}), bf16[128,2,384]{2,1,0:T(2,128)(2,1)S(1)}, u32[]{:S(2)}, u32[]{:S(2)}) async-start(bf16[128,2,384]{2,1,0:T(2,128)(2,1)} %copy.125), calls=%async_computation.11 | async-start | bytes 393216 | tf_op jit(solution)/shard_map/all_to_all | solution.py:178
  297.4 2.9 fusion
  300.2 16.7 %all-to-all-done.11 = bf16[128,2,384]{2,1,0:T(2,128)(2,1)S(1)} async-done(((bf16[128,2,384]{2,1,0:T(2,128)(2,1)}), bf16[128,2,384]{2,1,0:T(2,128)(2,1)S(1)}, u32[]{:S(2)}, u32[]{:S(2)}) %all-to-all-start.11) | async-done | bytes 196640 | tf_op jit(solution)/shard_map/all_to_all | solution.py:178
  317.0 0.8 gather_fusion
  317.9 0.6 add_convert_fusion.1
  (101 shorter events, 9.8 us)
Async XLA Ops:
  0.6 273.2 %copy-start = (bf16[1,1536,128]{2,1,0:T(8,128)(2,1)S(1)}, bf16[1,1536,128]{2,1,0:T(8,128)(2,1)}, u32[]{:S(2)}) copy-start(bf16[1,1536,128]{2,1,0:T(8,128)(2,1)} %param.29) | copy-start | bytes 1179652
  56.0 0.7 copy-start.5
  56.7 0.7 copy-start.6
  56.7 1.2 copy-start.7
  57.4 1.0 copy-start.8
  103.4 9.9 %copy-start.10 = (f32[384]{0:T(512)S(1)}, f32[384]{0:T(512)}, u32[]{:S(2)}) copy-start(f32[384]{0:T(512)} %param.23) | copy-start | bytes 4612
  108.3 12.5 %copy-start.1 = (bf16[15,3,128,128]{3,2,1,0:T(8,128)(2,1)S(1)}, bf16[15,3,128,128]{3,2,1,0:T(8,128)(2,1)}, u32[]{:S(2)}) copy-start(bf16[15,3,128,128]{3,2,1,0:T(8,128)(2,1)} %param.17) | copy-start | bytes 4423684
  109.1 11.1 %all-to-all-start.4 = ((f32[4,15,4,384]{3,2,1,0:T(4,128)}), f32[4,15,4,384]{3,2,1,0:T(4,128)S(1)}, u32[]{:S(2)}, u32[]{:S(2)}) async-start(f32[4,15,4,384]{3,2,1,0:T(4,128)} %copy.111), calls=%async_computation.4 | async-start | bytes 737280 | tf_op jit(solution)/shard_map/all_to_all | solution.py:44
  120.7 4.1 %copy-start.13 = (f32[128]{0:T(128)S(1)}, f32[128]{0:T(128)}, u32[]{:S(2)}) copy-start(f32[128]{0:T(128)} %param.24) | copy-start | bytes 1540
  120.7 8.5 %copy-start.11 = (s32[15,6]{0,1:T(8,128)S(1)}, s32[15,6]{0,1:T(8,128)}, u32[]{:S(2)}) copy-start(s32[15,6]{0,1:T(8,128)} %param.27) | copy-start | bytes 1084
  125.7 18.1 %all-to-all-start.5 = ((bf16[16,1,15,384]{3,2,1,0:T(8,128)(2,1)}), bf16[16,1,15,384]{3,2,1,0:T(8,128)(2,1)S(1)}, u32[]{:S(2)}, u32[]{:S(2)}) async-start(bf16[16,1,15,384]{3,2,1,0:T(8,128)(2,1)} %stack.46), calls=%async_computation.5 | async-start | bytes 393216 | tf_op jit(solution)/shard_map/all_to_all | solution.py:13
  144.8 12.6 %all-to-all-start.6 = ((bf16[4,16,15,384]{3,1,2,0:T(8,128)(2,1)}), bf16[4,16,15,384]{3,1,2,0:T(8,128)(2,1)S(1)}, u32[]{:S(2)}, u32[]{:S(2)}) async-start(bf16[4,16,15,384]{3,1,2,0:T(8,128)(2,1)} %stack.47), calls=%async_computation.6 | async-start | bytes 1474560 | tf_op jit(solution)/shard_map/all_to_all | solution.py:13
  149.2 8.5 %copy-start.14 = (s32[90]{0:T(128)}, s32[90]{0:T(128)S(1)}, u32[]{:S(2)}) copy-start(s32[90]{0:T(128)S(1)} %select_reduce_fusion) | copy-start | bytes 1084
  168.9 10.3 %copy-start.4 = (bf16[1,128,1536]{2,1,0:T(8,128)(2,1)S(1)}, bf16[1,128,1536]{2,1,0:T(8,128)(2,1)}, u32[]{:S(2)}) copy-start(bf16[1,128,1536]{2,1,0:T(8,128)(2,1)} %param.31) | copy-start | bytes 1179652
  170.8 42.0 %all-to-all-start.8 = ((bf16[128,15,12]{1,2,0:T(8,128)(2,1)}), bf16[128,15,12]{1,2,0:T(8,128)(2,1)S(1)}, u32[]{:S(2)}, u32[]{:S(2)}) async-start(bf16[128,15,12]{1,2,0:T(8,128)(2,1)} %copy.116), calls=%async_computation.8 | async-start | bytes 1048576 | tf_op jit(solution)/shard_map/all_to_all | solution.py:131
  189.1 42.8 %copy-start.3 = (bf16[15,1536]{1,0:T(8,128)(2,1)S(1)}, bf16[15,1536]{1,0:T(8,128)(2,1)}, u32[]{:S(2)}) copy-start(bf16[15,1536]{1,0:T(8,128)(2,1)} %param.16) | copy-start | bytes 138244
  189.1 43.0 %copy-start.9 = (f32[1536]{0:T(1024)S(1)}, f32[1536]{0:T(1024)}, u32[]{:S(2)}) copy-start(f32[1536]{0:T(1024)} %param.26) | copy-start | bytes 18436
  212.8 20.8 %all-to-all-start.10 = ((bf16[4,2,24576]{2,1,0:T(2,128)(2,1)}), bf16[4,2,24576]{2,1,0:T(2,128)(2,1)S(1)}, u32[]{:S(2)}, u32[]{:S(2)}) async-start(bf16[4,2,24576]{2,1,0:T(2,128)(2,1)} %reshape.237), calls=%async_computation.10 | async-start | bytes 786432 | tf_op jit(solution)/shard_map/all_to_all | solution.py:158
  233.6 28.5 %all-to-all-start.9 = ((bf16[128,2,384]{2,1,0:T(2,128)(2,1)}), bf16[128,2,384]{2,1,0:T(2,128)(2,1)S(1)}, u32[]{:S(2)}, u32[]{:S(2)}) async-start(bf16[128,2,384]{2,1,0:T(2,128)(2,1)} %constant_dynamic-slice_fusion), calls=%async_computation.9 | async-start | bytes 393216 | tf_op jit(solution)/shard_map/all_to_all | solution.py:161
  243.1 31.1 %copy-start.16 = (bf16[1,1536,128]{2,1,0:T(8,128)(2,1)S(1)}, bf16[1,1536,128]{2,1,0:T(8,128)(2,1)}, u32[]{:S(2)}) copy-start(bf16[1,1536,128]{2,1,0:T(8,128)(2,1)} %param.30) | copy-start | bytes 1179652
  274.2 23.0 %copy-start.12 = (f32[15,6]{0,1:T(8,128)S(1)}, f32[15,6]{0,1:T(8,128)}, u32[]{:S(2)}) copy-start(f32[15,6]{0,1:T(8,128)} %param.28) | copy-start | bytes 1084
  274.2 23.1 %copy-start.15 = (s32[90]{0:T(128)S(1)}, s32[90]{0:T(128)}, u32[]{:S(2)}) copy-start(s32[90]{0:T(128)} %copy-done.14) | copy-start | bytes 1084
  274.2 23.1 %copy-start.2 = (bf16[15,3,128,128]{3,2,1,0:T(8,128)(2,1)S(1)}, bf16[15,3,128,128]{3,2,1,0:T(8,128)(2,1)}, u32[]{:S(2)}) copy-start(bf16[15,3,128,128]{3,2,1,0:T(8,128)(2,1)} %param.17) | copy-start | bytes 4423684
  285.5 31.4 %all-to-all-start.11 = ((bf16[128,2,384]{2,1,0:T(2,128)(2,1)}), bf16[128,2,384]{2,1,0:T(2,128)(2,1)S(1)}, u32[]{:S(2)}, u32[]{:S(2)}) async-start(bf16[128,2,384]{2,1,0:T(2,128)(2,1)} %copy.125), calls=%async_computation.11 | async-start | bytes 393216 | tf_op jit(solution)/shard_map/all_to_all | solution.py:178
